TPU v7x, 32 devices: a whole 2x2x4 slice. The times are simulated.
32 devices in a mesh: fs: 16 (over z, y, x), tp: 2 (over core).
Axes of the slice: x: 2, y: 2, z: 4, core: 2. Of those that a mesh axis runs over, the one named last changes fastest.
Arguments:
- tokens: bfloat16 [2048, 2048], P('fs'), may hold values from -6 to 6
- norm_gain: float32 [2048], replicated, may hold values from 0.1 to 1.9
- w_query: bfloat16 [2048, 1024], P('fs', 'tp'), may hold values from -0.125 to 0.125
- w_key: bfloat16 [2048, 1024], P('fs', 'tp'), may hold values from -0.125 to 0.125
- w_value: bfloat16 [2048, 2048], P('fs', 'tp'), may hold values from -0.125 to 0.125
- w_gate: bfloat16 [2048, 2048], P('fs', 'tp'), may hold values from -0.125 to 0.125
- mixer_gain: float32 [2048], P('tp'), may hold values from 0.1 to 1.9
- w_out: bfloat16 [2048, 2048], P('tp', 'fs'), may hold values from -0.125 to 0.125
- channel_gain: float32 [2048], replicated, may hold values from 0.1 to 1.9
- w_left: bfloat16 [2048, 3072], P('fs', 'tp'), may hold values from -0.125 to 0.125
- w_right: bfloat16 [2048, 3072], P('fs', 'tp'), may hold values from -0.125 to 0.125
- taps_left: float32 [3, 3072], P(None, 'tp'), may hold values from -3.5 to 3.5
- taps_right: float32 [3, 3072], P(None, 'tp'), may hold values from -3.5 to 3.5
- w_down: bfloat16 [3072, 2048], P('tp', 'fs'), may hold values from -0.109375 to 0.109375
Outputs:
- layer_out: bfloat16 [2048, 2048], P('fs')
All inputs are finite; a program needn't handle non-finite values.
Results may differ from a plain program's by a relative error of at most 0.018.
Values may be sent and summed in bfloat16 or wider, within the bound.
A program may use at most 64 MiB of HBM per device.

v0:
```python
import jax
import jax.numpy as jnp
from jax import lax
from jax.sharding import PartitionSpec as P

DK = 128
DV = 256
BLOCK = 128
highest = lax.Precision.HIGHEST


def scale_rows(rows_in, gain_vec):
    floats = rows_in.astype(jnp.float32)
    factor = lax.rsqrt(jnp.mean(floats * floats, axis=-1, keepdims=True) + 1e-06)
    return (floats * factor * gain_vec).astype(jnp.bfloat16)


def decays(first_head, count):
    head_ids = first_head + jnp.arange(count, dtype=jnp.float32)
    return jnp.log(1.0 - 2.0 ** (-5.0 - head_ids))


def rotate(heads_in, positions):
    width = heads_in.shape[-1]
    half = width // 2
    freqs = 10000.0 ** (-jnp.arange(half, dtype=jnp.float32) / half)
    angles = positions[:, None] * freqs[None, :]
    cosine = jnp.cos(angles)
    sine = jnp.sin(angles)
    first_half = heads_in[..., :half]
    second_half = heads_in[..., half:]
    return jnp.concatenate(
        [first_half * cosine - second_half * sine, first_half * sine + second_half * cosine],
        axis=-1,
    )


def retention(queries, keys_in, values_in, log_gamma):
    head_count, length, key_width = queries.shape
    value_width = values_in.shape[-1]
    blocks = length // BLOCK
    queries = queries.reshape(head_count, blocks, BLOCK, key_width)
    keys_in = keys_in.reshape(head_count, blocks, BLOCK, key_width)
    values_in = values_in.reshape(head_count, blocks, BLOCK, value_width)
    offsets = jnp.arange(BLOCK, dtype=jnp.float32)
    distance = offsets[:, None] - offsets[None, :]
    weights = jnp.where(
        distance >= 0, jnp.exp(log_gamma[:, None, None] * jnp.maximum(distance, 0.0)), 0.0
    )
    scores = jnp.einsum("hbnd,hbmd->hbnm", queries, keys_in, precision=highest) * weights[:, None]
    inner = jnp.einsum("hbnm,hbme->hbne", scores, values_in, precision=highest)
    key_weight = jnp.exp(log_gamma[:, None] * (BLOCK - 1 - offsets)[None, :])
    contrib = jnp.einsum(
        "hbjd,hbje->hbde", keys_in * key_weight[:, None, :, None], values_in, precision=highest
    )
    block_decay = jnp.exp(log_gamma * BLOCK)[:, None, None]

    def advance(state, contrib_block):
        return (state * block_decay + contrib_block, state)

    _, states = lax.scan(
        advance,
        jnp.zeros((head_count, key_width, value_width), jnp.float32),
        jnp.moveaxis(contrib, 1, 0),
    )
    states = jnp.moveaxis(states, 0, 1)
    query_weight = jnp.exp(log_gamma[:, None] * (offsets + 1.0)[None, :])
    carried = (
        jnp.einsum("hbnd,hbde->hbne", queries, states, precision=highest)
        * query_weight[:, None, :, None]
    )
    return (inner + carried).reshape(head_count, length, value_width)


def head_norm(retained):
    return retained * lax.rsqrt(jnp.mean(retained * retained, axis=-1, keepdims=True) + 1e-06)


def causal_taps(values_in, taps):
    length = values_in.shape[-2]
    padded = jnp.pad(values_in.astype(jnp.float32), ((taps.shape[0] - 1, 0), (0, 0)))
    result = padded[0:length] * taps[0]
    for tap_index in range(1, taps.shape[0]):
        result = result + padded[tap_index : tap_index + length] * taps[tap_index]
    return result


def fold_single(source, weight_piece):
    return jnp.dot(source, weight_piece, preferred_element_type=jnp.float32)


def collect_single(source, weight):
    return fold_single(source, lax.all_gather(weight, "fs", axis=0, tiled=True))


def body(
    tokens,
    norm_gain,
    w_query,
    w_key,
    w_value,
    w_gate,
    mixer_gain,
    w_out,
    channel_gain,
    w_left,
    w_right,
    taps_left,
    taps_right,
    w_down,
):
    length = tokens.shape[0]
    normed = scale_rows(tokens, norm_gain)
    queries = collect_single(normed, w_query)
    keys_proj = collect_single(normed, w_key)
    values_proj = collect_single(normed, w_value)
    gates = collect_single(normed, w_gate)
    queries = queries.astype(jnp.bfloat16)
    keys_proj = keys_proj.astype(jnp.bfloat16)
    values_proj = values_proj.astype(jnp.bfloat16)
    gates = gates.astype(jnp.bfloat16)
    heads_here = w_query.shape[1] // DK
    first_head = (lax.axis_index("tp") * heads_here).astype(jnp.float32)
    log_gamma = decays(first_head, heads_here)
    positions = jnp.arange(length, dtype=jnp.float32)

    def split_heads(rows_in, width):
        return rows_in.astype(jnp.float32).reshape(length, heads_here, width).transpose(1, 0, 2)

    retained = head_norm(
        retention(
            rotate(split_heads(queries, DK), positions),
            rotate(split_heads(keys_proj, DK), positions),
            split_heads(values_proj, DV),
            log_gamma,
        )
    )
    retained = retained.transpose(1, 0, 2).reshape(length, heads_here * DV)
    hidden = (retained * mixer_gain * jax.nn.silu(gates.astype(jnp.float32))).astype(jnp.bfloat16)
    rows_own = length // lax.axis_size("tp")
    first_row = lax.axis_index("tp") * rows_own
    out_whole = lax.all_gather(w_out, "fs", axis=1, tiled=True)
    mixer_total = lax.psum_scatter(
        jnp.dot(hidden, out_whole, preferred_element_type=jnp.float32).astype(jnp.bfloat16),
        "tp",
        scatter_dimension=0,
        tiled=True,
    ).astype(jnp.float32)
    residual = lax.dynamic_slice_in_dim(tokens, first_row, rows_own, 0)
    middle_own = (residual.astype(jnp.float32) + mixer_total).astype(jnp.bfloat16)
    middle = lax.all_gather(middle_own, "tp", axis=0, tiled=True)
    normed_mid = scale_rows(middle, channel_gain)
    left = collect_single(normed_mid, w_left)
    right = collect_single(normed_mid, w_right)
    left = left.astype(jnp.bfloat16)
    right = right.astype(jnp.bfloat16)
    gated = (jax.nn.silu(causal_taps(left, taps_left)) * causal_taps(right, taps_right)).astype(
        jnp.bfloat16
    )
    down_whole = lax.all_gather(w_down, "fs", axis=1, tiled=True)
    channel_part = jnp.dot(gated, down_whole, preferred_element_type=jnp.float32)
    channel_total = lax.psum(channel_part.astype(jnp.bfloat16), "tp").astype(jnp.float32)
    return (middle.astype(jnp.float32) + channel_total).astype(jnp.bfloat16)


def solution(mesh):
    placed = (
        P("fs", None),
        P(),
        P("fs", "tp"),
        P("fs", "tp"),
        P("fs", "tp"),
        P("fs", "tp"),
        P("tp"),
        P("tp", "fs"),
        P(),
        P("fs", "tp"),
        P("fs", "tp"),
        P(None, "tp"),
        P(None, "tp"),
        P("tp", "fs"),
    )
    return jax.shard_map(body, mesh=mesh, in_specs=placed, out_specs=P("fs", None), check_vma=False)
```

profile of v0, /device:TPU:0, one launch (start us, length us, event | category | flops | bytes accessed | tf_op | source)
XLA Modules:
  0.0 730.4 jit_solution(5038678450189377104)
XLA Ops:
  6.5 0.7 all-gather.11.cloned.1.call-update
  7.3 0.0 all-gather.9.cloned.1.call-start
  7.3 0.7 all-gather.9.cloned.1.call-update
  8.0 0.0 all-gather.13.cloned.1.call-start
  8.1 0.7 all-gather.13.cloned.1.call-update
  8.8 0.5 all-gather.15.cloned.1.call-update
  9.3 0.0 all-gather.17.cloned.1.call-start
  9.4 0.5 all-gather.17.cloned.1.call-update
  9.9 0.0 reduce-scatter.2.cloned.1.call-start
  10.1 1.2 fusion.7
  11.3 0.1 multiply_exponential_fusion
  11.4 0.1 multiply_exponential_fusion.1
  11.5 0.3 fusion.49
  11.7 61.5 %all-gather.11.cloned.1.call-done = bf16[2048,512]{1,0:T(8,128)(2,1)} async-done(((bf16[128,512]{1,0:T(8,128)(2,1)}), bf16[2048,512]{1,0:T(8,128)(2,1)}) %all-gather.11.cloned.1.call-update) | async-done | bytes 2097168 | tf_op jit(solution)/shard_map/all_gather | solution.py:93
  73.2 2.3 fusion.4
  75.5 59.7 %all-gather.9.cloned.1.call-done = bf16[2048,512]{1,0:T(8,128)(2,1)} async-done(((bf16[128,512]{1,0:T(8,128)(2,1)}), bf16[2048,512]{1,0:T(8,128)(2,1)}) %all-gather.9.cloned.1.call-update) | async-done | bytes 2097168 | tf_op jit(solution)/shard_map/all_gather | solution.py:93
  135.2 2.1 fusion.6
  137.3 0.3 multiply_subtract_fusion
  137.6 0.4 fusion.42
  138.1 0.7 convolution_multiply_fusion
  138.8 73.6 %all-gather.13.cloned.1.call-done = bf16[2048,1024]{1,0:T(8,128)(2,1)} async-done(((bf16[128,1024]{1,0:T(8,128)(2,1)}), bf16[2048,1024]{1,0:T(8,128)(2,1)}) %all-gather.13.cloned.1.call-update) | async-done | bytes 4194320 | tf_op jit(solution)/shard_map/all_gather | solution.py:93
  212.4 2.9 convolution_convert_fusion.5
  215.4 0.5 multiply_reduce_fusion
  215.8 0.2 fusion.25
  216.1 0.2 copy.21
  216.3 0.2 copy.22
  216.5 72.8 %all-gather.15.cloned.1.call-done = bf16[2048,1024]{1,0:T(8,128)(2,1)} async-done(((bf16[128,1024]{1,0:T(8,128)(2,1)}), bf16[2048,1024]{1,0:T(8,128)(2,1)}) %all-gather.15.cloned.1.call-update) | async-done | bytes 4194320 | tf_op jit(solution)/shard_map/all_gather | solution.py:93
  289.3 89.9 %all-gather.17.cloned.1.call-done = bf16[1024,2048]{1,0:T(8,128)(2,1)} async-done(((bf16[1024,128]{1,0:T(8,128)(2,1)}), bf16[1024,2048]{1,0:T(8,128)(2,1)}) %all-gather.17.cloned.1.call-update) | async-done | bytes 4194320 | tf_op jit(solution)/shard_map/all_gather | solution.py:142
  379.2 5.7 convolution_convert_fusion.1
  384.9 0.0 all-gather.19.cloned.1.call-start
  384.9 0.7 all-gather.19.cloned.1.call-update
  385.6 0.0 all-gather.21.cloned.1.call-start
  385.7 0.7 all-gather.21.cloned.1.call-update
  386.4 0.7 all-gather.23.cloned.1.call-update
  387.1 0.0 all-reduce.4.cloned.1.call-start
  387.2 0.1 slice_reduce_fusion.2
  387.3 3.9 reduce-scatter.2.cloned.1.call-done
  391.2 1.0 add_convert_fusion
  392.2 2.2 all_gather.32
  394.4 0.2 fusion.10
  394.5 93.9 %all-gather.19.cloned.1.call-done = bf16[2048,1536]{1,0:T(8,128)(2,1)} async-done(((bf16[128,1536]{1,0:T(8,128)(2,1)}), bf16[2048,1536]{1,0:T(8,128)(2,1)}) %all-gather.19.cloned.1.call-update) | async-done | bytes 6291472 | tf_op jit(solution)/shard_map/all_gather | solution.py:93
  488.5 3.8 fusion.1
  492.3 90.9 %all-gather.21.cloned.1.call-done = bf16[2048,1536]{1,0:T(8,128)(2,1)} async-done(((bf16[128,1536]{1,0:T(8,128)(2,1)}), bf16[2048,1536]{1,0:T(8,128)(2,1)}) %all-gather.21.cloned.1.call-update) | async-done | bytes 6291472 | tf_op jit(solution)/shard_map/all_gather | solution.py:93
  583.2 3.8 fusion
  587.0 112.5 %all-gather.23.cloned.1.call-done = bf16[1536,2048]{1,0:T(8,128)(2,1)} async-done(((bf16[1536,128]{1,0:T(8,128)(2,1)}), bf16[1536,2048]{1,0:T(8,128)(2,1)}) %all-gather.23.cloned.1.call-update) | async-done | bytes 6291472 | tf_op jit(solution)/shard_map/all_gather | solution.py:160
  699.5 5.1 convolution_convert_fusion
  704.6 16.9 %all-reduce.4.cloned.1.call-done = bf16[128,2048]{1,0:T(8,128)(2,1)} async-done(((bf16[128,2048]{1,0:T(8,128)(2,1)}), bf16[128,2048]{1,0:T(8,128)(2,1)}) %all-reduce.4.cloned.1.call-update) | async-done | bytes 524304 | tf_op jit(solution)/shard_map/psum | solution.py:162
  721.6 2.0 fusion.13
  (27 shorter events, 0.3 us)
Async XLA Ops:
  6.5 128.7 %copy-start = (bf16[128,2048]{1,0:T(8,128)(2,1)S(1)}, bf16[128,2048]{1,0:T(8,128)(2,1)}, u32[]{:S(2)}) copy-start(bf16[128,2048]{1,0:T(8,128)(2,1)} %param.14) | copy-start | bytes 1572868
  6.5 128.7 %copy-start.1 = (f32[2048]{0:T(1024)S(1)}, f32[2048]{0:T(1024)}, u32[]{:S(2)}) copy-start(f32[2048]{0:T(1024)} %param.15) | copy-start | bytes 24580
  6.5 66.7 %all-gather.11.cloned.1.call-start = ((), (), s32[]{:S(2)}) async-start(), calls=%async_computation.2 | async-start | bytes 2228224 | tf_op jit(solution)/shard_map/all_gather | solution.py:93
  7.3 128.0 %all-gather.9.cloned.1.call-start = ((), (), s32[]{:S(2)}) async-start(), calls=%async_computation.1 | async-start | bytes 2228224 | tf_op jit(solution)/shard_map/all_gather | solution.py:93
  8.0 204.4 %all-gather.13.cloned.1.call-start = ((), (), s32[]{:S(2)}) async-start(), calls=%async_computation.3 | async-start | bytes 4456448 | tf_op jit(solution)/shard_map/all_gather | solution.py:93
  8.7 280.5 %all-gather.15.cloned.1.call-start = ((), (), s32[]{:S(2)}) async-start(), calls=%async_computation.4 | async-start | bytes 4456448 | tf_op jit(solution)/shard_map/all_gather | solution.py:93
  9.3 369.8 %all-gather.17.cloned.1.call-start = ((), (), s32[]{:S(2)}) async-start(), calls=%async_computation.5 | async-start | bytes 4456448 | tf_op jit(solution)/shard_map/all_gather | solution.py:142
  9.9 381.2 %reduce-scatter.2.cloned.1.call-start = ((), (), s32[]{:S(2)}) async-start(), calls=%async_computation.6 | async-start | bytes 786432 | tf_op jit(solution)/shard_map/reduce_scatter | solution.py:143
  138.8 240.4 %copy-start.5 = (f32[1024]{0:T(1024)S(1)}, f32[1024]{0:T(1024)}, u32[]{:S(2)}) copy-start(f32[1024]{0:T(1024)} %param.20) | copy-start | bytes 12292
  216.5 170.7 %copy-start.3 = (f32[3,1536]{1,0:T(4,128)S(1)}, f32[3,1536]{1,0:T(4,128)}, u32[]{:S(2)}) copy-start(f32[3,1536]{1,0:T(4,128)} %param.26) | copy-start | bytes 55300
  216.5 170.7 %copy-start.4 = (f32[3,1536]{1,0:T(4,128)S(1)}, f32[3,1536]{1,0:T(4,128)}, u32[]{:S(2)}) copy-start(f32[3,1536]{1,0:T(4,128)} %param.25) | copy-start | bytes 55300
  216.5 272.0 %copy-start.2 = (f32[2048]{0:T(1024)S(1)}, f32[2048]{0:T(1024)}, u32[]{:S(2)}) copy-start(f32[2048]{0:T(1024)} %param.22) | copy-start | bytes 24580
  384.9 103.6 %all-gather.19.cloned.1.call-start = ((), (), s32[]{:S(2)}) async-start(), calls=%async_computation.7 | async-start | bytes 6684672 | tf_op jit(solution)/shard_map/all_gather | solution.py:93
  385.6 197.6 %all-gather.21.cloned.1.call-start = ((), (), s32[]{:S(2)}) async-start(), calls=%async_computation.8 | async-start | bytes 6684672 | tf_op jit(solution)/shard_map/all_gather | solution.py:93
  386.4 313.1 %all-gather.23.cloned.1.call-start = ((), (), s32[]{:S(2)}) async-start(), calls=%async_computation.9 | async-start | bytes 6684672 | tf_op jit(solution)/shard_map/all_gather | solution.py:160
  387.1 334.4 %all-reduce.4.cloned.1.call-start = ((), (), s32[]{:S(2)}) async-start(), calls=%async_computation.10 | async-start | bytes 1048576 | tf_op jit(solution)/shard_map/psum | solution.py:162
Sparse Core Ops, SparseCore 0:
  10.1 63.0 all-gather.10
  76.0 59.1 all-gather.8
  138.0 74.3 all-gather.12
  215.0 74.1 all-gather.14
  291.8 87.3 all-gather.16
  385.0 6.0 reduce-scatter.1
  393.9 94.5 all-gather.18
  491.3 91.9 all-gather.20
  585.9 113.5 all-gather.22
  704.8 16.7 all-reduce.3
where the time goes:
time: 731 us; the launch traced here: 730 us
  waiting for transfers between devices  681 us (93%)
  matrix products  27.3 us (4%)
  between operations  13.7 us (2%)
    all_gather x6, waiting for transfers between devices, collect_single(): return fold_single(source, lax.all_gather(weight, 'fs', axis=0, tiled=True))  452 us
    all_gather x1, waiting for transfers between devices, body(): down_whole = lax.all_gather(w_down, 'fs', axis=1, tiled=True)  112 us
    all_gather x1, waiting for transfers between devices, body(): out_whole = lax.all_gather(w_out, 'fs', axis=1, tiled=True)  89.9 us
    psum x1, waiting for transfers between devices, body(): lax.psum(channel_part.astype(jnp.bfloat16), 'tp').astype(jnp.float32)  16.9 us
    dot_general x5, matrix products, fold_single(): return jnp.dot(source, weight_piece, preferred_element_type=jnp.float32)  14.9 us
  transfers between devices with their start and end apart: 10, of which 10 were waited for; matrix products, arithmetic and copies ran while one was open for 3% of the time, Pallas kernels for 0%

commit v1 on v0

--- a/solution.py
+++ b/solution.py
@@ -139,7 +139,12 @@
     hidden = (retained * mixer_gain * jax.nn.silu(gates.astype(jnp.float32))).astype(jnp.bfloat16)
     rows_own = length // lax.axis_size("tp")
     first_row = lax.axis_index("tp") * rows_own
-    out_whole = lax.all_gather(w_out, "fs", axis=1, tiled=True)
+    ring = [w_out]
+    for hop in range(15):
+        ring.append(lax.ppermute(ring[-1], "fs", [(dev, (dev + 1) % 16) for dev in range(16)]))
+    out_whole = jnp.roll(
+        jnp.concatenate(ring[::-1], axis=1), (lax.axis_index("fs") + 1) * ring[0].shape[1], axis=1
+    )
     mixer_total = lax.psum_scatter(
         jnp.dot(hidden, out_whole, preferred_element_type=jnp.float32).astype(jnp.bfloat16),
         "tp",

time: 731 us -> 663 us (0.907)
  waiting for transfers between devices: 681 us -> 575 us
  local copies, waits for them, and re-layouts: 0.56 us -> 32.4 us
    all_gather x6, waiting for transfers between devices: 452 us -> 247 us  [collect_single(): return fold_single(source, lax.all_gather(weight, 'fs', axis=0, tiled=True))]
    ppermute x0 -> x15, waiting for transfers between devices: none -> 190 us  [body(): lax.ppermute(ring[-1], 'fs', [(dev, (dev + 1) % 16) for dev in range(16)])]
    all_gather x1 -> x0, waiting for transfers between devices: 89.9 us -> none  [body(): out_whole = lax.all_gather(w_out, 'fs', axis=1, tiled=True)]
    unnamed x12 -> x61, local copies, waits for them, and re-layouts: 0.03 us -> 31.1 us
  transfers between devices with their start and end apart: 10 -> 24, of which waited for: 10 -> 21; matrix products, arithmetic and copies ran while one was open for 3% -> 8% of each run, Pallas kernels for 0% -> 0%
where the time goes in v1:
time: 663 us; the launch traced here: 662 us
  waiting for transfers between devices  575 us (87%)
  local copies, waits for them, and re-layouts  32.4 us (5%)
  matrix products  27.9 us (4%)
  between operations  13.5 us (2%)
  other arithmetic  7.94 us (1%)
    all_gather x6, waiting for transfers between devices, collect_single(): return fold_single(source, lax.all_gather(weight, 'fs', axis=0, tiled=True))  247 us
    ppermute x15, waiting for transfers between devices, body(): lax.ppermute(ring[-1], 'fs', [(dev, (dev + 1) % 16) for dev in range(16)])  190 us
    all_gather x1, waiting for transfers between devices, body(): down_whole = lax.all_gather(w_down, 'fs', axis=1, tiled=True)  112 us
    unnamed x61, local copies, waits for them, and re-layouts  31.1 us
    psum x1, waiting for transfers between devices, body(): lax.psum(channel_part.astype(jnp.bfloat16), 'tp').astype(jnp.float32)  16.9 us
    dot_general x5, matrix products, fold_single(): return jnp.dot(source, weight_piece, preferred_element_type=jnp.float32)  14.8 us
  transfers between devices with their start and end apart: 24, of which 21 were waited for; matrix products, arithmetic and copies ran while one was open for 8% of the time, Pallas kernels for 0%

profile of v1, /device:TPU:0, one launch (start us, length us, event | category | flops | bytes accessed | tf_op | source)
XLA Modules:
  0.0 662.4 jit_solution(38680455617118590)
XLA Ops:
  8.8 3.0 collective-permute-start
  11.8 10.5 %collective-permute-done = bf16[1024,128]{1,0:T(8,128)(2,1)S(1)} collective-permute-done((bf16[1024,128]{1,0:T(8,128)(2,1)}, bf16[1024,128]{1,0:T(8,128)(2,1)S(1)}, u32[]{:S(2)}, u32[]{:S(2)}) %collective-permute-start) | collective-permute-done | bytes 262176 | tf_op jit(solution)/shard_map/ppermute | solution.py:144
  22.3 13.8 %collective-permute-done.1 = bf16[1024,128]{1,0:T(8,128)(2,1)S(1)} collective-permute-done((bf16[1024,128]{1,0:T(8,128)(2,1)S(1)}, bf16[1024,128]{1,0:T(8,128)(2,1)S(1)}, u32[]{:S(2)}, u32[]{:S(2)}) %collective-permute-start.1) | collective-permute-done | bytes 262176 | tf_op jit(solution)/shard_map/ppermute | solution.py:144
  36.2 14.3 %collective-permute-done.2 = bf16[1024,128]{1,0:T(8,128)(2,1)S(1)} collective-permute-done((bf16[1024,128]{1,0:T(8,128)(2,1)S(1)}, bf16[1024,128]{1,0:T(8,128)(2,1)S(1)}, u32[]{:S(2)}, u32[]{:S(2)}) %collective-permute-start.2) | collective-permute-done | bytes 262176 | tf_op jit(solution)/shard_map/ppermute | solution.py:144
  50.4 10.0 %collective-permute-done.3 = bf16[1024,128]{1,0:T(8,128)(2,1)S(1)} collective-permute-done((bf16[1024,128]{1,0:T(8,128)(2,1)S(1)}, bf16[1024,128]{1,0:T(8,128)(2,1)S(1)}, u32[]{:S(2)}, u32[]{:S(2)}) %collective-permute-start.3) | collective-permute-done | bytes 262176 | tf_op jit(solution)/shard_map/ppermute | solution.py:144
  60.4 16.8 %collective-permute-done.4 = bf16[1024,128]{1,0:T(8,128)(2,1)S(1)} collective-permute-done((bf16[1024,128]{1,0:T(8,128)(2,1)S(1)}, bf16[1024,128]{1,0:T(8,128)(2,1)S(1)}, u32[]{:S(2)}, u32[]{:S(2)}) %collective-permute-start.4) | collective-permute-done | bytes 262176 | tf_op jit(solution)/shard_map/ppermute | solution.py:144
  77.2 11.5 %collective-permute-done.5 = bf16[1024,128]{1,0:T(8,128)(2,1)S(1)} collective-permute-done((bf16[1024,128]{1,0:T(8,128)(2,1)S(1)}, bf16[1024,128]{1,0:T(8,128)(2,1)S(1)}, u32[]{:S(2)}, u32[]{:S(2)}) %collective-permute-start.5) | collective-permute-done | bytes 262176 | tf_op jit(solution)/shard_map/ppermute | solution.py:144
  88.7 14.5 %collective-permute-done.6 = bf16[1024,128]{1,0:T(8,128)(2,1)S(1)} collective-permute-done((bf16[1024,128]{1,0:T(8,128)(2,1)S(1)}, bf16[1024,128]{1,0:T(8,128)(2,1)S(1)}, u32[]{:S(2)}, u32[]{:S(2)}) %collective-permute-start.6) | collective-permute-done | bytes 262176 | tf_op jit(solution)/shard_map/ppermute | solution.py:144
  103.2 12.0 %collective-permute-done.7 = bf16[1024,128]{1,0:T(8,128)(2,1)S(1)} collective-permute-done((bf16[1024,128]{1,0:T(8,128)(2,1)S(1)}, bf16[1024,128]{1,0:T(8,128)(2,1)S(1)}, u32[]{:S(2)}, u32[]{:S(2)}) %collective-permute-start.7) | collective-permute-done | bytes 262176 | tf_op jit(solution)/shard_map/ppermute | solution.py:144
  115.2 13.7 %collective-permute-done.8 = bf16[1024,128]{1,0:T(8,128)(2,1)S(1)} collective-permute-done((bf16[1024,128]{1,0:T(8,128)(2,1)S(1)}, bf16[1024,128]{1,0:T(8,128)(2,1)S(1)}, u32[]{:S(2)}, u32[]{:S(2)}) %collective-permute-start.8) | collective-permute-done | bytes 262176 | tf_op jit(solution)/shard_map/ppermute | solution.py:144
  129.1 15.7 %collective-permute-done.9 = bf16[1024,128]{1,0:T(8,128)(2,1)S(1)} collective-permute-done((bf16[1024,128]{1,0:T(8,128)(2,1)S(1)}, bf16[1024,128]{1,0:T(8,128)(2,1)S(1)}, u32[]{:S(2)}, u32[]{:S(2)}) %collective-permute-start.9) | collective-permute-done | bytes 262176 | tf_op jit(solution)/shard_map/ppermute | solution.py:144
  144.8 1.2 fusion.12
  146.0 9.9 %collective-permute-done.10 = bf16[1024,128]{1,0:T(8,128)(2,1)S(1)} collective-permute-done((bf16[1024,128]{1,0:T(8,128)(2,1)S(1)}, bf16[1024,128]{1,0:T(8,128)(2,1)S(1)}, u32[]{:S(2)}, u32[]{:S(2)}) %collective-permute-start.10) | collective-permute-done | bytes 262176 | tf_op jit(solution)/shard_map/ppermute | solution.py:144
  156.5 9.4 %collective-permute-done.11 = bf16[1024,128]{1,0:T(8,128)(2,1)S(1)} collective-permute-done((bf16[1024,128]{1,0:T(8,128)(2,1)S(1)}, bf16[1024,128]{1,0:T(8,128)(2,1)S(1)}, u32[]{:S(2)}, u32[]{:S(2)}) %collective-permute-start.11) | collective-permute-done | bytes 262176 | tf_op jit(solution)/shard_map/ppermute | solution.py:144
  166.0 14.7 %collective-permute-done.12 = bf16[1024,128]{1,0:T(8,128)(2,1)S(1)} collective-permute-done((bf16[1024,128]{1,0:T(8,128)(2,1)S(1)}, bf16[1024,128]{1,0:T(8,128)(2,1)S(1)}, u32[]{:S(2)}, u32[]{:S(2)}) %collective-permute-start.12) | collective-permute-done | bytes 262176 | tf_op jit(solution)/shard_map/ppermute | solution.py:144
  182.1 13.5 %collective-permute-done.13 = bf16[1024,128]{1,0:T(8,128)(2,1)} collective-permute-done((bf16[1024,128]{1,0:T(8,128)(2,1)S(1)}, bf16[1024,128]{1,0:T(8,128)(2,1)}, u32[]{:S(2)}, u32[]{:S(2)}) %collective-permute-start.13) | collective-permute-done | bytes 262176 | tf_op jit(solution)/shard_map/ppermute | solution.py:144
  195.7 0.9 fusion.54
  196.5 9.3 %collective-permute-done.14 = bf16[1024,128]{1,0:T(8,128)(2,1)} collective-permute-done((bf16[1024,128]{1,0:T(8,128)(2,1)}, bf16[1024,128]{1,0:T(8,128)(2,1)}, u32[]{:S(2)}, u32[]{:S(2)}) %collective-permute-start.14) | collective-permute-done | bytes 262176 | tf_op jit(solution)/shard_map/ppermute | solution.py:144
  205.9 1.8 constant_dynamic-update-slice_fusion.31
  207.7 1.7 constant_dynamic-update-slice_fusion.30
  209.4 1.7 constant_dynamic-update-slice_fusion.29
  211.1 1.7 constant_dynamic-update-slice_fusion.28
  212.8 1.7 constant_dynamic-update-slice_fusion.27
  217.6 0.8 constant_dynamic-update-slice_fusion.22
  221.3 0.8 constant_dynamic-update-slice_fusion.17
  222.9 1.7 constant_dynamic-update-slice_fusion.15
  224.6 1.7 constant_dynamic-update-slice_fusion.14
  226.3 0.8 constant_dynamic-update-slice_fusion.13
  227.8 0.8 constant_dynamic-update-slice_fusion.11
  228.6 0.8 constant_dynamic-update-slice_fusion.10
  237.0 2.1 fusion.9
  239.1 2.1 fusion.11
  241.3 1.1 multiply_subtract_fusion
  242.8 1.5 convolution_multiply_fusion
  244.3 3.0 convolution_convert_fusion.4
  248.4 62.8 %all-gather.14.cloned.1.call-done = bf16[2048,1024]{1,0:T(8,128)(2,1)} async-done(((bf16[128,1024]{1,0:T(8,128)(2,1)}), bf16[2048,1024]{1,0:T(8,128)(2,1)}) %all-gather.14.cloned.1.call-update) | async-done | bytes 4194320 | tf_op jit(solution)/shard_map/all_gather | solution.py:93
  311.3 5.7 fusion.2
  319.2 4.4 reduce-scatter.2.cloned.1.call-done
  323.7 1.0 add_convert_fusion
  324.7 2.4 all_gather.28
  327.2 93.6 %all-gather.16.cloned.1.call-done = bf16[2048,1536]{1,0:T(8,128)(2,1)} async-done(((bf16[128,1536]{1,0:T(8,128)(2,1)}), bf16[2048,1536]{1,0:T(8,128)(2,1)}) %all-gather.16.cloned.1.call-update) | async-done | bytes 6291472 | tf_op jit(solution)/shard_map/all_gather | solution.py:93
  420.8 3.8 fusion.6
  424.7 90.9 %all-gather.18.cloned.1.call-done = bf16[2048,1536]{1,0:T(8,128)(2,1)} async-done(((bf16[128,1536]{1,0:T(8,128)(2,1)}), bf16[2048,1536]{1,0:T(8,128)(2,1)}) %all-gather.18.cloned.1.call-update) | async-done | bytes 6291472 | tf_op jit(solution)/shard_map/all_gather | solution.py:93
  515.6 3.8 fusion.5
  519.4 112.5 %all-gather.20.cloned.1.call-done = bf16[1536,2048]{1,0:T(8,128)(2,1)} async-done(((bf16[1536,128]{1,0:T(8,128)(2,1)}), bf16[1536,2048]{1,0:T(8,128)(2,1)}) %all-gather.20.cloned.1.call-update) | async-done | bytes 6291472 | tf_op jit(solution)/shard_map/all_gather | solution.py:165
  631.9 5.1 convolution_convert_fusion
  637.0 16.9 %all-reduce.4.cloned.1.call-done = bf16[128,2048]{1,0:T(8,128)(2,1)} async-done(((bf16[128,2048]{1,0:T(8,128)(2,1)}), bf16[128,2048]{1,0:T(8,128)(2,1)}) %all-reduce.4.cloned.1.call-update) | async-done | bytes 524304 | tf_op jit(solution)/shard_map/psum | solution.py:167
  653.9 2.0 fusion.18
  (104 shorter events, 23.5 us)
Async XLA Ops:
  6.5 215.6 %copy-start.1 = (bf16[1024,128]{1,0:T(8,128)(2,1)S(1)}, bf16[1024,128]{1,0:T(8,128)(2,1)}, u32[]{:S(2)}) copy-start(bf16[1024,128]{1,0:T(8,128)(2,1)} %param.21) | copy-start | bytes 786436
  6.5 230.5 %all-gather.10.cloned.1.call-start = ((), (), s32[]{:S(2)}) async-start(), calls=%async_computation.2 | async-start | bytes 2228224 | tf_op jit(solution)/shard_map/all_gather | solution.py:93
  7.3 231.9 %all-gather.8.cloned.1.call-start = ((), (), s32[]{:S(2)}) async-start(), calls=%async_computation.1 | async-start | bytes 2228224 | tf_op jit(solution)/shard_map/all_gather | solution.py:93
  8.0 236.3 %all-gather.12.cloned.1.call-start = ((), (), s32[]{:S(2)}) async-start(), calls=%async_computation.3 | async-start | bytes 4456448 | tf_op jit(solution)/shard_map/all_gather | solution.py:93
  8.7 302.5 %all-gather.14.cloned.1.call-start = ((), (), s32[]{:S(2)}) async-start(), calls=%async_computation.4 | async-start | bytes 4456448 | tf_op jit(solution)/shard_map/all_gather | solution.py:93
  8.8 13.5 %collective-permute-start = (bf16[1024,128]{1,0:T(8,128)(2,1)}, bf16[1024,128]{1,0:T(8,128)(2,1)S(1)}, u32[]{:S(2)}, u32[]{:S(2)}) collective-permute-start(bf16[1024,128]{1,0:T(8,128)(2,1)} %param.21), channel_id=1, source_target_pairs={{0,2},{2,4},{4,6},{6,8},{8,10},{10,12},{12,14},{14,16},{16,18},{18... | collective-permute-start | bytes 786440 | tf_op jit(solution)/shard_map/ppermute | solution.py:144
  22.3 13.8 %collective-permute-start.1 = (bf16[1024,128]{1,0:T(8,128)(2,1)S(1)}, bf16[1024,128]{1,0:T(8,128)(2,1)S(1)}, u32[]{:S(2)}, u32[]{:S(2)}) collective-permute-start(bf16[1024,128]{1,0:T(8,128)(2,1)S(1)} %collective-permute-done), channel_id=1, source_target_pairs={{0,2},{2,4},{4,6},{6,8},{8,10},{10,12},{12,14},{14,16},{16,18},{18... | collective-permute-start | bytes 786440 | tf_op jit(solution)/shard_map/ppermute | solution.py:144
  36.1 14.3 %collective-permute-start.2 = (bf16[1024,128]{1,0:T(8,128)(2,1)S(1)}, bf16[1024,128]{1,0:T(8,128)(2,1)S(1)}, u32[]{:S(2)}, u32[]{:S(2)}) collective-permute-start(bf16[1024,128]{1,0:T(8,128)(2,1)S(1)} %collective-permute-done.1), channel_id=1, source_target_pairs={{0,2},{2,4},{4,6},{6,8},{8,10},{10,12},{12,14},{14,16},{16,18},{18... | collective-permute-start | bytes 786440 | tf_op jit(solution)/shard_map/ppermute | solution.py:144
  50.4 10.0 %collective-permute-start.3 = (bf16[1024,128]{1,0:T(8,128)(2,1)S(1)}, bf16[1024,128]{1,0:T(8,128)(2,1)S(1)}, u32[]{:S(2)}, u32[]{:S(2)}) collective-permute-start(bf16[1024,128]{1,0:T(8,128)(2,1)S(1)} %collective-permute-done.2), channel_id=1, source_target_pairs={{0,2},{2,4},{4,6},{6,8},{8,10},{10,12},{12,14},{14,16},{16,18},{18... | collective-permute-start | bytes 786440 | tf_op jit(solution)/shard_map/ppermute | solution.py:144
  60.4 16.8 %collective-permute-start.4 = (bf16[1024,128]{1,0:T(8,128)(2,1)S(1)}, bf16[1024,128]{1,0:T(8,128)(2,1)S(1)}, u32[]{:S(2)}, u32[]{:S(2)}) collective-permute-start(bf16[1024,128]{1,0:T(8,128)(2,1)S(1)} %collective-permute-done.3), channel_id=1, source_target_pairs={{0,2},{2,4},{4,6},{6,8},{8,10},{10,12},{12,14},{14,16},{16,18},{18... | collective-permute-start | bytes 786440 | tf_op jit(solution)/shard_map/ppermute | solution.py:144
  77.2 11.5 %collective-permute-start.5 = (bf16[1024,128]{1,0:T(8,128)(2,1)S(1)}, bf16[1024,128]{1,0:T(8,128)(2,1)S(1)}, u32[]{:S(2)}, u32[]{:S(2)}) collective-permute-start(bf16[1024,128]{1,0:T(8,128)(2,1)S(1)} %collective-permute-done.4), channel_id=1, source_target_pairs={{0,2},{2,4},{4,6},{6,8},{8,10},{10,12},{12,14},{14,16},{16,18},{18... | collective-permute-start | bytes 786440 | tf_op jit(solution)/shard_map/ppermute | solution.py:144
  88.7 14.5 %collective-permute-start.6 = (bf16[1024,128]{1,0:T(8,128)(2,1)S(1)}, bf16[1024,128]{1,0:T(8,128)(2,1)S(1)}, u32[]{:S(2)}, u32[]{:S(2)}) collective-permute-start(bf16[1024,128]{1,0:T(8,128)(2,1)S(1)} %collective-permute-done.5), channel_id=1, source_target_pairs={{0,2},{2,4},{4,6},{6,8},{8,10},{10,12},{12,14},{14,16},{16,18},{18... | collective-permute-start | bytes 786440 | tf_op jit(solution)/shard_map/ppermute | solution.py:144
  103.2 12.0 %collective-permute-start.7 = (bf16[1024,128]{1,0:T(8,128)(2,1)S(1)}, bf16[1024,128]{1,0:T(8,128)(2,1)S(1)}, u32[]{:S(2)}, u32[]{:S(2)}) collective-permute-start(bf16[1024,128]{1,0:T(8,128)(2,1)S(1)} %collective-permute-done.6), channel_id=1, source_target_pairs={{0,2},{2,4},{4,6},{6,8},{8,10},{10,12},{12,14},{14,16},{16,18},{18... | collective-permute-start | bytes 786440 | tf_op jit(solution)/shard_map/ppermute | solution.py:144
  115.2 13.7 %collective-permute-start.8 = (bf16[1024,128]{1,0:T(8,128)(2,1)S(1)}, bf16[1024,128]{1,0:T(8,128)(2,1)S(1)}, u32[]{:S(2)}, u32[]{:S(2)}) collective-permute-start(bf16[1024,128]{1,0:T(8,128)(2,1)S(1)} %collective-permute-done.7), channel_id=1, source_target_pairs={{0,2},{2,4},{4,6},{6,8},{8,10},{10,12},{12,14},{14,16},{16,18},{18... | collective-permute-start | bytes 786440 | tf_op jit(solution)/shard_map/ppermute | solution.py:144
  129.0 15.8 %collective-permute-start.9 = (bf16[1024,128]{1,0:T(8,128)(2,1)S(1)}, bf16[1024,128]{1,0:T(8,128)(2,1)S(1)}, u32[]{:S(2)}, u32[]{:S(2)}) collective-permute-start(bf16[1024,128]{1,0:T(8,128)(2,1)S(1)} %collective-permute-done.8), channel_id=1, source_target_pairs={{0,2},{2,4},{4,6},{6,8},{8,10},{10,12},{12,14},{14,16},{16,18},{18... | collective-permute-start | bytes 786440 | tf_op jit(solution)/shard_map/ppermute | solution.py:144
  129.0 194.6 %reduce-scatter.2.cloned.1.call-start = ((), (), s32[]{:S(2)}) async-start(), calls=%async_computation.5 | async-start | bytes 786432 | tf_op jit(solution)/shard_map/reduce_scatter | solution.py:148
  144.7 11.2 %collective-permute-start.10 = (bf16[1024,128]{1,0:T(8,128)(2,1)S(1)}, bf16[1024,128]{1,0:T(8,128)(2,1)S(1)}, u32[]{:S(2)}, u32[]{:S(2)}) collective-permute-start(bf16[1024,128]{1,0:T(8,128)(2,1)S(1)} %collective-permute-done.9), channel_id=1, source_target_pairs={{0,2},{2,4},{4,6},{6,8},{8,10},{10,12},{12,14},{14,16},{16,18},{18... | collective-permute-start | bytes 786440 | tf_op jit(solution)/shard_map/ppermute | solution.py:144
  155.9 39.7 %copy-start.2 = (bf16[1024,128]{1,0:T(8,128)(2,1)}, bf16[1024,128]{1,0:T(8,128)(2,1)S(1)}, u32[]{:S(2)}) copy-start(bf16[1024,128]{1,0:T(8,128)(2,1)S(1)} %collective-permute-done.10) | copy-start | bytes 786436
  155.9 10.0 %collective-permute-start.11 = (bf16[1024,128]{1,0:T(8,128)(2,1)S(1)}, bf16[1024,128]{1,0:T(8,128)(2,1)S(1)}, u32[]{:S(2)}, u32[]{:S(2)}) collective-permute-start(bf16[1024,128]{1,0:T(8,128)(2,1)S(1)} %collective-permute-done.10), channel_id=1, source_target_pairs={{0,2},{2,4},{4,6},{6,8},{8,10},{10,12},{12,14},{14,16},{16,18},{18... | collective-permute-start | bytes 786440 | tf_op jit(solution)/shard_map/ppermute | solution.py:144
  165.9 29.8 %copy-start.4 = (bf16[1024,128]{1,0:T(8,128)(2,1)}, bf16[1024,128]{1,0:T(8,128)(2,1)S(1)}, u32[]{:S(2)}) copy-start(bf16[1024,128]{1,0:T(8,128)(2,1)S(1)} %collective-permute-done.11) | copy-start | bytes 786436
  165.9 14.8 %collective-permute-start.12 = (bf16[1024,128]{1,0:T(8,128)(2,1)S(1)}, bf16[1024,128]{1,0:T(8,128)(2,1)S(1)}, u32[]{:S(2)}, u32[]{:S(2)}) collective-permute-start(bf16[1024,128]{1,0:T(8,128)(2,1)S(1)} %collective-permute-done.11), channel_id=1, source_target_pairs={{0,2},{2,4},{4,6},{6,8},{8,10},{10,12},{12,14},{14,16},{16,18},{18... | collective-permute-start | bytes 786440 | tf_op jit(solution)/shard_map/ppermute | solution.py:144
  165.9 29.7 %copy-start.12 = (f32[4]{0:T(128)}, f32[4]{0:T(128)S(1)}, u32[]{:S(2)}) copy-start(f32[4]{0:T(128)S(1)} %subtract_log_fusion) | copy-start | bytes 52
  180.7 0.7 copy-start.6
  181.4 14.2 %collective-permute-start.13 = (bf16[1024,128]{1,0:T(8,128)(2,1)S(1)}, bf16[1024,128]{1,0:T(8,128)(2,1)}, u32[]{:S(2)}, u32[]{:S(2)}) collective-permute-start(bf16[1024,128]{1,0:T(8,128)(2,1)S(1)} %collective-permute-done.12), channel_id=1, source_target_pairs={{0,2},{2,4},{4,6},{6,8},{8,10},{10,12},{12,14},{14,16},{16,18},{18... | collective-permute-start | bytes 786440 | tf_op jit(solution)/shard_map/ppermute | solution.py:144
  195.6 10.3 %collective-permute-start.14 = (bf16[1024,128]{1,0:T(8,128)(2,1)}, bf16[1024,128]{1,0:T(8,128)(2,1)}, u32[]{:S(2)}, u32[]{:S(2)}) collective-permute-start(bf16[1024,128]{1,0:T(8,128)(2,1)} %collective-permute-done.13), channel_id=1, source_target_pairs={{0,2},{2,4},{4,6},{6,8},{8,10},{10,12},{12,14},{14,16},{16,18},{18... | collective-permute-start | bytes 786440 | tf_op jit(solution)/shard_map/ppermute | solution.py:144
  195.6 30.7 %copy-start.7 = (bf16[1024,128]{1,0:T(8,128)(2,1)S(1)}, bf16[1024,128]{1,0:T(8,128)(2,1)}, u32[]{:S(2)}) copy-start(bf16[1024,128]{1,0:T(8,128)(2,1)} %copy-done.6) | copy-start | bytes 786436
  196.5 30.5 %copy-start.5 = (bf16[1024,128]{1,0:T(8,128)(2,1)S(1)}, bf16[1024,128]{1,0:T(8,128)(2,1)}, u32[]{:S(2)}) copy-start(bf16[1024,128]{1,0:T(8,128)(2,1)} %copy-done.4) | copy-start | bytes 786436
  196.5 31.3 %copy-start.3 = (bf16[1024,128]{1,0:T(8,128)(2,1)S(1)}, bf16[1024,128]{1,0:T(8,128)(2,1)}, u32[]{:S(2)}) copy-start(bf16[1024,128]{1,0:T(8,128)(2,1)} %copy-done.2) | copy-start | bytes 786436
  196.5 40.5 %copy-start = (bf16[128,2048]{1,0:T(8,128)(2,1)S(1)}, bf16[128,2048]{1,0:T(8,128)(2,1)}, u32[]{:S(2)}) copy-start(bf16[128,2048]{1,0:T(8,128)(2,1)} %param.14) | copy-start | bytes 1572868
  196.5 40.5 %copy-start.8 = (f32[2048]{0:T(1024)S(1)}, f32[2048]{0:T(1024)}, u32[]{:S(2)}) copy-start(f32[2048]{0:T(1024)} %param.15) | copy-start | bytes 24580
  229.4 14.8 %copy-start.13 = (f32[128]{0:T(128)S(1)}, f32[128]{0:T(128)}, u32[]{:S(2)}) copy-start(f32[128]{0:T(128)} %add_rsqrt_fusion.1) | copy-start | bytes 1540
  241.2 70.0 %copy-start.14 = (f32[1024]{0:T(1024)S(1)}, f32[1024]{0:T(1024)}, u32[]{:S(2)}) copy-start(f32[1024]{0:T(1024)} %param.20) | copy-start | bytes 12292
  247.8 71.3 %copy-start.10 = (f32[3,1536]{1,0:T(4,128)S(1)}, f32[3,1536]{1,0:T(4,128)}, u32[]{:S(2)}) copy-start(f32[3,1536]{1,0:T(4,128)} %param.26) | copy-start | bytes 55300
  247.8 71.3 %copy-start.11 = (f32[3,1536]{1,0:T(4,128)S(1)}, f32[3,1536]{1,0:T(4,128)}, u32[]{:S(2)}) copy-start(f32[3,1536]{1,0:T(4,128)} %param.25) | copy-start | bytes 55300
  248.0 172.8 %copy-start.9 = (f32[2048]{0:T(1024)S(1)}, f32[2048]{0:T(1024)}, u32[]{:S(2)}) copy-start(f32[2048]{0:T(1024)} %param.22) | copy-start | bytes 24580
  317.0 103.9 %all-gather.16.cloned.1.call-start = ((), (), s32[]{:S(2)}) async-start(), calls=%async_computation.6 | async-start | bytes 6684672 | tf_op jit(solution)/shard_map/all_gather | solution.py:93
  317.6 198.0 %all-gather.18.cloned.1.call-start = ((), (), s32[]{:S(2)}) async-start(), calls=%async_computation.7 | async-start | bytes 6684672 | tf_op jit(solution)/shard_map/all_gather | solution.py:93
  318.3 313.6 %all-gather.20.cloned.1.call-start = ((), (), s32[]{:S(2)}) async-start(), calls=%async_computation.8 | async-start | bytes 6684672 | tf_op jit(solution)/shard_map/all_gather | solution.py:165
  319.1 334.8 %all-reduce.4.cloned.1.call-start = ((), (), s32[]{:S(2)}) async-start(), calls=%async_computation.9 | async-start | bytes 1048576 | tf_op jit(solution)/shard_map/psum | solution.py:167
Sparse Core Ops, SparseCore 0:
  10.1 71.8 all-gather.9
  84.8 68.7 all-gather.7
  156.4 78.0 all-gather.11
  237.0 74.1 all-gather.13
  317.1 6.5 reduce-scatter.1
  326.3 94.4 all-gather.15
  423.6 91.9 all-gather.17
  518.3 113.5 all-gather.19
  637.1 16.7 all-reduce.3
